TPU v7x, 32 devices: a whole 2x2x4 slice. The times are simulated.
32 devices in a mesh: sp: 16 (over z, y, core), tp: 2 (over x).
Axes of the slice: x: 2, y: 2, z: 4, core: 2. Of those that a mesh axis runs over, the one named last changes fastest.
Arguments:
- queries: bfloat16 [8192, 1024], P('sp', 'tp'), may hold values from -160 to 160
- keys: bfloat16 [8192, 256], P('sp', 'tp'), may hold values from -5 to 5
- values: bfloat16 [8192, 256], P('sp', 'tp'), may hold values from -6 to 6
- doc_ids: int32 [8192], P('sp'), may hold values from 0 to 7, never falling along the last dimension, each value on 1 to 2048 neighbouring positions
- sink_logit: float32 [16], P('tp'), may hold values from 1 to 6
- w_out: bfloat16 [1024, 2048], P('tp'), may hold values from -0.1875 to 0.1875
- residual: bfloat16 [8192, 2048], P(('sp', 'tp')), may hold values from -6 to 6
- ffn_gain: float32 [2048], replicated, may hold values from 0.1 to 1.9
- expert_ids: int32 [8192, 8], P(('sp', 'tp')), may hold values from 0 to 15, all different within a row; in each aligned block of 128 rows (0 to 127, 128 to 255, ...) at most 96 rows name the same one
- expert_weight: float32 [8192, 8], P(('sp', 'tp')), may hold values from 0.2 to 2
- exp_gate: bfloat16 [16, 2048, 512], P('sp'), may hold values from -0.125 to 0.125
- exp_up: bfloat16 [16, 2048, 512], P('sp'), may hold values from -0.125 to 0.125
- exp_down: bfloat16 [16, 512, 2048], P('sp'), may hold values from -0.25 to 0.25
- shared_gate: bfloat16 [2048, 512], P(None, 'tp'), may hold values from -0.125 to 0.125
- shared_up: bfloat16 [2048, 512], P(None, 'tp'), may hold values from -0.125 to 0.125
- shared_down: bfloat16 [512, 2048], P('tp'), may hold values from -0.25 to 0.25
Outputs:
- output: bfloat16 [8192, 2048], P(('sp', 'tp'))
Inputs may be any that keep to these rules, and one draw needn't show every extreme that they name: `doc_ids`: never falling along the sequence; every document holds at most 2048 positions, and one holds exactly that many. `expert_ids`: each row names 8 different experts. In each aligned block of 128 rows no expert is named by more than 96 rows, and in some blocks one expert is named by exactly 96 rows.
All inputs are finite; a program needn't handle non-finite values.
Results may differ from a plain program's by a relative error of at most 0.018.
Values may be sent and summed in bfloat16 or wider, within the bound.
A program may use at most 128 MiB of HBM per device.

v0:
```python
import jax
import jax.numpy as jnp
from jax import lax
from jax.sharding import PartitionSpec as P

HD = 64
WINDOW = 128


norm_eps = 1e-06


def extended(cells, sides, width):
    for axis, dim in sides:
        count = lax.axis_size(axis)
        ends = count - 1
        head = lax.slice_in_dim(cells, 0, width, axis=dim)
        tail = lax.slice_in_dim(cells, cells.shape[dim] - width, cells.shape[dim], axis=dim)
        cells = jnp.concatenate(
            [
                lax.ppermute(tail, axis, [(i, (i + 1) % count) for i in range(ends)]),
                cells,
                lax.ppermute(head, axis, [((i + 1) % count, i) for i in range(ends)]),
            ],
            axis=dim,
        )
    return cells


def band_blocks(padded, width):
    span_count = padded.shape[0] // width - 2
    shaped = padded.reshape((span_count + 2, width) + padded.shape[1:])
    return jnp.concatenate(
        [
            shaped[0:span_count:2],
            shaped[1 : span_count + 1 : 2],
            shaped[2 : span_count + 2 : 2],
            shaped[3 : span_count + 3 : 2],
        ],
        axis=1,
    )


def attend(queries, ext_keys, ext_values, ext_marks, own_marks, sink_logit):
    tok_count = queries.shape[0]
    head_count = sink_logit.shape[0]
    key_heads = ext_keys.shape[1] // HD
    group_size = head_count // key_heads
    query_span = 2 * WINDOW
    block_count = tok_count // query_span
    query_blocks = queries.reshape(block_count, query_span, key_heads, group_size, HD)
    key_blocks = band_blocks(ext_keys, WINDOW).reshape(block_count, 4 * WINDOW, key_heads, HD)
    value_blocks = band_blocks(ext_values, WINDOW).reshape(block_count, 4 * WINDOW, key_heads, HD)
    mark_blocks = band_blocks(ext_marks, WINDOW)
    query_marks = own_marks.reshape(block_count, query_span)
    scores = jnp.einsum(
        "nqkgd,nmkd->nkgqm", query_blocks, key_blocks, preferred_element_type=jnp.float32
    ) * HD ** (-0.5)
    offset = (
        jnp.arange(query_span, dtype=jnp.int32)[:, None]
        - jnp.arange(4 * WINDOW, dtype=jnp.int32)[None, :]
        + WINDOW
    )
    allowed = (jnp.abs(offset) <= WINDOW)[None] & (
        mark_blocks[:, None, :] == query_marks[:, :, None]
    )
    scores = jnp.where(allowed[:, None, None], scores, -jnp.inf)
    sink_term = sink_logit.reshape(key_heads, group_size)[None, :, :, None, None]
    row_max = jnp.maximum(jnp.max(scores, axis=-1, keepdims=True), sink_term)
    exp_scores = jnp.exp(scores - row_max)
    attn_probs = (
        exp_scores / (jnp.sum(exp_scores, axis=-1, keepdims=True) + jnp.exp(sink_term - row_max))
    ).astype(jnp.bfloat16)
    result = jnp.einsum(
        "nkgqm,nmkd->nqkgd", attn_probs, value_blocks, preferred_element_type=jnp.float32
    )
    return result.astype(jnp.bfloat16).reshape(tok_count, head_count * HD)


def slot_index(routing, half_rows, slot_cap, expert_count):
    blocks = routing.shape[0] // half_rows
    flat_ids = routing.reshape(blocks, half_rows * routing.shape[1])
    onehot = (
        flat_ids[:, :, None] == jnp.arange(expert_count, dtype=jnp.int32)[None, None, :]
    ).astype(jnp.int32)
    slot_rank = jnp.sum(jnp.cumsum(onehot, axis=1) * onehot, axis=-1) - 1
    slot_place = (
        flat_ids * (blocks * slot_cap)
        + jnp.arange(blocks, dtype=jnp.int32)[:, None] * slot_cap
        + slot_rank
    )
    return slot_place.reshape(-1)


def pack_rows(normed, slot_place, expert_count, per_expert):
    assign_count = slot_place.shape[0]
    top_count = assign_count // normed.shape[0]
    source = (
        jnp.full((expert_count * per_expert,), normed.shape[0], jnp.int32)
        .at[slot_place]
        .set(jnp.arange(assign_count, dtype=jnp.int32) // top_count)
    )
    packed = jnp.take(normed, source, axis=0, mode="fill", fill_value=0)
    return packed.reshape(expert_count, per_expert, normed.shape[1])


def run_expert(arrived, gate_w, up_w, down_w):
    flat_rows = arrived.reshape(-1, arrived.shape[-1])
    hidden = (
        jax.nn.silu(jnp.dot(flat_rows, gate_w, preferred_element_type=jnp.float32))
        * jnp.dot(flat_rows, up_w, preferred_element_type=jnp.float32)
    ).astype(jnp.bfloat16)
    return (
        jnp.dot(hidden, down_w, preferred_element_type=jnp.float32)
        .astype(jnp.bfloat16)
        .reshape(arrived.shape)
    )


def combine_rows(returned, slot_place, weights):
    picked = returned.reshape(-1, returned.shape[-1])[slot_place].reshape(
        weights.shape + (returned.shape[-1],)
    )
    return jnp.sum(weights[:, :, None] * picked.astype(jnp.float32), axis=1)


def shards(
    queries,
    keys,
    values,
    doc_ids,
    sink_logit,
    w_out,
    residual,
    ffn_gain,
    expert_ids,
    expert_weight,
    exp_gate,
    exp_up,
    exp_down,
    shared_gate,
    shared_up,
    shared_down,
):
    marks = (doc_ids + 1).astype(jnp.bfloat16)
    ext_keys, ext_values, ext_marks = (
        extended(keys, (("sp", 0),), WINDOW),
        extended(values, (("sp", 0),), WINDOW),
        extended(marks, (("sp", 0),), WINDOW),
    )
    attended = attend(queries, ext_keys, ext_values, ext_marks, marks, sink_logit)
    row_count = residual.shape[0]
    mixed = lax.psum_scatter(
        jnp.dot(attended, w_out, preferred_element_type=jnp.float32).astype(jnp.bfloat16),
        "tp",
        scatter_dimension=0,
        tiled=True,
    ).astype(jnp.float32)
    resid = (residual.astype(jnp.float32) + mixed).astype(jnp.bfloat16)
    resid_f = resid.astype(jnp.float32)
    normed = (
        resid_f
        * lax.rsqrt(jnp.mean(resid_f * resid_f, axis=-1, keepdims=True) + norm_eps)
        * ffn_gain
    ).astype(jnp.bfloat16)
    shard_rows = lax.all_gather(normed, "tp", axis=0, tiled=True)
    hidden = (
        jax.nn.silu(jnp.dot(shard_rows, shared_gate, preferred_element_type=jnp.float32))
        * jnp.dot(shard_rows, shared_up, preferred_element_type=jnp.float32)
    ).astype(jnp.bfloat16)
    partial_out = jnp.dot(hidden, shared_down, preferred_element_type=jnp.float32)
    shared_terms = lax.optimization_barrier(partial_out.astype(jnp.bfloat16)).astype(jnp.float32)
    shared_out = lax.psum_scatter(
        shared_terms.astype(jnp.bfloat16), "tp", scatter_dimension=0, tiled=True
    ).astype(jnp.float32)
    expert_count = lax.axis_size("sp") * exp_gate.shape[0]
    top_count = expert_ids.shape[1]
    half_rows = row_count // 2
    slot_cap = min(half_rows, max(2, 3 * half_rows * top_count // (2 * expert_count)))
    halves_out = []
    for half_index in range(2):
        first_row = half_index * half_rows
        part_ids = expert_ids[first_row : first_row + half_rows]
        part_rows = normed[first_row : first_row + half_rows]
        part_weight = expert_weight[first_row : first_row + half_rows]
        slot_place = slot_index(part_ids, half_rows, slot_cap, expert_count)
        packed = pack_rows(part_rows, slot_place, expert_count, slot_cap)
        returned = lax.all_to_all(
            run_expert(
                lax.all_to_all(packed, "sp", split_axis=0, concat_axis=0, tiled=True),
                exp_gate[0],
                exp_up[0],
                exp_down[0],
            ),
            "sp",
            split_axis=0,
            concat_axis=0,
            tiled=True,
        )
        halves_out.append(combine_rows(returned, slot_place, part_weight))
    routed = jnp.concatenate(halves_out, axis=0)
    return (resid.astype(jnp.float32) + shared_out + routed).astype(jnp.bfloat16)


def solution(mesh):
    placed = (
        P("sp", "tp"),
        P("sp", "tp"),
        P("sp", "tp"),
        P("sp"),
        P("tp"),
        P("tp", None),
        P(("sp", "tp"), None),
        P(),
        P(("sp", "tp"), None),
        P(("sp", "tp"), None),
        P("sp", None, None),
        P("sp", None, None),
        P("sp", None, None),
        P(None, "tp"),
        P(None, "tp"),
        P("tp", None),
    )
    return jax.shard_map(
        shards, mesh=mesh, in_specs=placed, out_specs=P(("sp", "tp"), None), check_vma=False
    )
```

profile of v0, /device:TPU:13, one launch (start us, length us, event | category | flops | bytes accessed | tf_op | source)
XLA Modules:
  0.0 713.5 jit_solution(18196577709892937796)
XLA Ops:
  7.4 3.7 collective-permute-start.2
  11.1 1.9 collective-permute-start.3
  13.0 1.4 fusion.52
  14.4 4.5 collective-permute-start.4
  19.0 1.9 collective-permute-start.5
  20.9 1.4 fusion.53
  22.3 4.5 collective-permute-start
  27.0 2.2 reshape.508
  29.9 1.9 collective-permute-start.1
  34.8 1.6 copy.65
  36.4 1.6 copy.66
  39.7 1.8 fusion.3
  41.5 1.8 fusion.2
  43.3 1.4 copy-done.1
  46.2 5.8 fusion.21
  52.7 2.6 convolution_convert_fusion.3
  55.6 4.5 reduce-window.14
  60.8 4.5 scatter_custom_fusion
  65.4 22.8 %reduce-scatter.3.cloned.1.call-done = bf16[256,2048]{1,0:T(8,128)(2,1)} async-done(((bf16[512,2048]{1,0:T(8,128)(2,1)}), bf16[256,2048]{1,0:T(8,128)(2,1)}) %reduce-scatter.3.cloned.1.call-update) | async-done | bytes 1048592 | tf_op jit(solution)/shard_map/reduce_scatter | solution.py:153
  88.2 1.6 fusion.7
  89.9 2.6 fusion.9
  92.5 1.3 fusion.49
  93.7 7.1 %gather_fusion.2 = bf16[1536,2048]{1,0:T(8,128)(2,1)} fusion(bf16[128,2048]{1,0:T(8,128)(2,1)S(1)} %get-tuple-element.6, s32[2048]{0:T(1024)S(1)} %pad_clamp_fusion.1), kind=kCustom, calls=%fused_computation.clone | custom fusion | bytes 12589056 | tf_op jit(solution)/shard_map/jit(_take)/gather | solution.py:103
  100.9 5.9 broadcast_select_fusion.1
  106.8 6.5 all-to-all-start
  113.5 4.5 reduce-window.16
  118.7 4.3 scatter_custom_fusion.1
  123.1 7.1 gather_fusion.3
  130.2 5.9 broadcast_select_fusion
  136.2 114.5 %all-to-all-done = bf16[16,96,2048]{2,1,0:T(8,128)(2,1)} async-done(((bf16[16,96,2048]{2,1,0:T(8,128)(2,1)}), bf16[16,96,2048]{2,1,0:T(8,128)(2,1)}, u32[]{:S(2)}, u32[]{:S(2)}) %all-to-all-start) | async-done | bytes 6291488 | tf_op jit(solution)/shard_map/all_to_all | solution.py:190
  250.7 4.8 all-to-all-start.2
  255.5 8.6 %fusion.18 = f32[1536,512]{1,0:T(8,128)} fusion(bf16[1536,2048]{1,0:T(8,128)(2,1)} %bitcast.18, bf16[1,2048,512]{2,1,0:T(8,128)(2,1)} %param.28), kind=kOutput, calls=%fused_computation.40 | convolution fusion | flops 3221225472 | bytes 11534336 | tf_op jit(solution)/shard_map/dot_general | solution.py:110
  264.1 11.8 %convolution_convert_fusion.1 = bf16[1536,2048]{1,0:T(8,128)(2,1)} fusion(bf16[1,512,2048]{2,1,0:T(8,128)(2,1)S(1)} %copy-done, bf16[1536,2048]{1,0:T(8,128)(2,1)} %bitcast.18, f32[1536,512]{1,0:T(8,128)} %fusion.18, bf16[1,2048,512]{2,1,0:T(8,128)(2,1)} %param.29), kind=kOutput, calls=%fused_computation.14 | convolution fusion | flops 6450315264 | bytes 19922944 | tf_op jit(solution)/shard_map/dot_general | solution.py:114
  275.8 117.0 %all-to-all-done.2 = bf16[16,96,2048]{2,1,0:T(8,128)(2,1)} async-done(((bf16[16,96,2048]{2,1,0:T(8,128)(2,1)}), bf16[16,96,2048]{2,1,0:T(8,128)(2,1)}, u32[]{:S(2)}, u32[]{:S(2)}) %all-to-all-start.2) | async-done | bytes 6291488 | tf_op jit(solution)/shard_map/all_to_all | solution.py:190
  392.9 5.1 all-to-all-start.1
  398.0 8.6 %fusion.16 = f32[1536,512]{1,0:T(8,128)} fusion(bf16[1536,2048]{1,0:T(8,128)(2,1)} %bitcast.32, bf16[1,2048,512]{2,1,0:T(8,128)(2,1)} %param.28), kind=kOutput, calls=%fused_computation.38 | convolution fusion | flops 3221225472 | bytes 11534336 | tf_op jit(solution)/shard_map/dot_general | solution.py:110
  406.6 11.7 %convolution_convert_fusion = bf16[1536,2048]{1,0:T(8,128)(2,1)} fusion(bf16[1,512,2048]{2,1,0:T(8,128)(2,1)S(1)} %copy-done, bf16[1536,2048]{1,0:T(8,128)(2,1)} %bitcast.32, f32[1536,512]{1,0:T(8,128)} %fusion.16, bf16[1,2048,512]{2,1,0:T(8,128)(2,1)} %param.29), kind=kOutput, calls=%fused_computation.13 | convolution fusion | flops 6450315264 | bytes 19922944 | tf_op jit(solution)/shard_map/dot_general | solution.py:114
  418.4 116.9 %all-to-all-done.1 = bf16[16,96,2048]{2,1,0:T(8,128)(2,1)} async-done(((bf16[16,96,2048]{2,1,0:T(8,128)(2,1)}), bf16[16,96,2048]{2,1,0:T(8,128)(2,1)}, u32[]{:S(2)}, u32[]{:S(2)}) %all-to-all-start.1) | async-done | bytes 6291488 | tf_op jit(solution)/shard_map/all_to_all | solution.py:188
  535.3 4.8 all-to-all-start.3
  540.8 34.2 %all-gather.2.cloned.1.call-done = bf16[512,2048]{1,0:T(8,128)(2,1)} async-done(((bf16[256,2048]{1,0:T(8,128)(2,1)}), bf16[512,2048]{1,0:T(8,128)(2,1)}) %all-gather.2.cloned.1.call-update) | async-done | bytes 2097168 | tf_op jit(solution)/shard_map/all_gather | solution.py:166
  575.0 2.6 fusion.57
  577.6 5.8 convolution_convert_fusion.2
  583.7 12.7 %gather_fusion = bf16[1024,2048]{1,0:T(8,128)(2,1)} fusion(bf16[1536,2048]{1,0:T(8,128)(2,1)} %bitcast.23, s32[1024]{0:T(1024)S(1)} %broadcast_clamp_fusion.1), kind=kCustom, calls=%fused_computation.2 | custom fusion | bytes 8392704 | tf_op jit(solution)/shard_map/gather | solution.py:121
  596.4 81.1 %all-to-all-done.3 = bf16[16,96,2048]{2,1,0:T(8,128)(2,1)} async-done(((bf16[16,96,2048]{2,1,0:T(8,128)(2,1)}), bf16[16,96,2048]{2,1,0:T(8,128)(2,1)}, u32[]{:S(2)}, u32[]{:S(2)}) %all-to-all-start.3) | async-done | bytes 6291488 | tf_op jit(solution)/shard_map/all_to_all | solution.py:188
  677.4 12.4 %gather_fusion.1 = bf16[1024,2048]{1,0:T(8,128)(2,1)} fusion(bf16[1536,2048]{1,0:T(8,128)(2,1)} %bitcast.34, s32[1024]{0:T(1024)S(1)} %broadcast_clamp_fusion), kind=kCustom, calls=%fused_computation.3 | custom fusion | bytes 8392704 | tf_op jit(solution)/shard_map/gather | solution.py:121
  689.9 7.6 %fusion.1 = f32[128,2048]{1,0:T(8,128)} fusion(bf16[1024,2048]{1,0:T(8,128)(2,1)} %gather_fusion, f32[128,8]{1,0:T(8,128)S(1)} %copy.45), kind=kLoop, calls=%fused_computation.9 | loop fusion | flops 6029312 | bytes 5246976 | tf_op jit(solution)/shard_map/reduce_sum | solution.py:124
  697.5 5.3 fusion
  702.8 3.7 fusion.11
  (108 shorter events, 11.4 us)
Async XLA Ops:
  6.5 257.5 %copy-start = (bf16[1,512,2048]{2,1,0:T(8,128)(2,1)S(1)}, bf16[1,512,2048]{2,1,0:T(8,128)(2,1)}, u32[]{:S(2)}) copy-start(bf16[1,512,2048]{2,1,0:T(8,128)(2,1)} %param.30) | copy-start | bytes 6291460
  6.5 81.7 %reduce-scatter.3.cloned.1.call-start = ((), (), s32[]{:S(2)}) async-start(), calls=%async_computation.6 | async-start | bytes 3145728 | tf_op jit(solution)/shard_map/reduce_scatter | solution.py:153
  7.4 22.5 %collective-permute-start.2 = (bf16[128]{0:T(256)(128)(2,1)S(1)}, bf16[128]{0:T(256)(128)(2,1)S(1)}, u32[]{:S(2)}, u32[]{:S(2)}) collective-permute-start(bf16[128]{0:T(256)(128)(2,1)S(1)} %get-tuple-element.26), channel_id=1, source_target_pairs={{0,2},{2,4},{4,6},{6,8},{8,10},{10,12},{12,14},{14,16},{16,18},{18... | collective-permute-start | bytes 776 | tf_op jit(solution)/shard_map/ppermute | solution.py:21
  11.1 20.8 %collective-permute-start.3 = (bf16[128]{0:T(256)(128)(2,1)S(1)}, bf16[128]{0:T(256)(128)(2,1)S(1)}, u32[]{:S(2)}, u32[]{:S(2)}) collective-permute-start(bf16[128]{0:T(256)(128)(2,1)S(1)} %get-tuple-element.27), channel_id=1, source_target_pairs={{2,0},{4,2},{6,4},{8,6},{10,8},{12,10},{14,12},{16,14},{18,16},{20... | collective-permute-start | bytes 776 | tf_op jit(solution)/shard_map/ppermute | solution.py:23
  14.4 17.8 %collective-permute-start.4 = (bf16[128,128]{1,0:T(8,128)(2,1)}, bf16[128,128]{1,0:T(8,128)(2,1)}, u32[]{:S(2)}, u32[]{:S(2)}) collective-permute-start(bf16[128,128]{1,0:T(8,128)(2,1)} %get-tuple-element.16), channel_id=1, source_target_pairs={{0,2},{2,4},{4,6},{6,8},{8,10},{10,12},{12,14},{14,16},{16,18},{18... | collective-permute-start | bytes 98312 | tf_op jit(solution)/shard_map/ppermute | solution.py:21
  19.0 13.3 %collective-permute-start.5 = (bf16[128,128]{1,0:T(8,128)(2,1)}, bf16[128,128]{1,0:T(8,128)(2,1)}, u32[]{:S(2)}, u32[]{:S(2)}) collective-permute-start(bf16[128,128]{1,0:T(8,128)(2,1)} %get-tuple-element.17), channel_id=1, source_target_pairs={{2,0},{4,2},{6,4},{8,6},{10,8},{12,10},{14,12},{16,14},{18,16},{20... | collective-permute-start | bytes 98312 | tf_op jit(solution)/shard_map/ppermute | solution.py:23
  22.3 22.5 %collective-permute-start = (bf16[128,128]{1,0:T(8,128)(2,1)}, bf16[128,128]{1,0:T(8,128)(2,1)}, u32[]{:S(2)}, u32[]{:S(2)}) collective-permute-start(bf16[128,128]{1,0:T(8,128)(2,1)} %get-tuple-element.18), channel_id=1, source_target_pairs={{0,2},{2,4},{4,6},{6,8},{8,10},{10,12},{12,14},{14,16},{16,18},{18... | collective-permute-start | bytes 98312 | tf_op jit(solution)/shard_map/ppermute | solution.py:21
  29.9 14.8 %collective-permute-start.1 = (bf16[128,128]{1,0:T(8,128)(2,1)}, bf16[128,128]{1,0:T(8,128)(2,1)}, u32[]{:S(2)}, u32[]{:S(2)}) collective-permute-start(bf16[128,128]{1,0:T(8,128)(2,1)} %get-tuple-element.19), channel_id=1, source_target_pairs={{2,0},{4,2},{6,4},{8,6},{10,8},{12,10},{14,12},{16,14},{18,16},{20... | collective-permute-start | bytes 98312 | tf_op jit(solution)/shard_map/ppermute | solution.py:23
  41.4 3.2 copy-start.1
  41.5 3.2 copy-start.5
  46.2 6.5 copy-start.9
  52.7 2.7 copy-start.7
  55.3 32.9 %copy-start.3 = (bf16[256,2048]{1,0:T(8,128)(2,1)S(1)}, bf16[256,2048]{1,0:T(8,128)(2,1)}, u32[]{:S(2)}) copy-start(bf16[256,2048]{1,0:T(8,128)(2,1)} %param.24) | copy-start | bytes 3145732
  55.3 34.6 %copy-start.6 = (f32[2048]{0:T(1024)S(1)}, f32[2048]{0:T(1024)}, u32[]{:S(2)}) copy-start(f32[2048]{0:T(1024)} %param.25) | copy-start | bytes 24580
  106.8 143.9 %all-to-all-start = ((bf16[16,96,2048]{2,1,0:T(8,128)(2,1)}), bf16[16,96,2048]{2,1,0:T(8,128)(2,1)}, u32[]{:S(2)}, u32[]{:S(2)}) async-start(bf16[16,96,2048]{2,1,0:T(8,128)(2,1)} %bitcast.114), calls=%async_computation.2 | async-start | bytes 12582912 | tf_op jit(solution)/shard_map/all_to_all | solution.py:190
  250.7 142.2 %all-to-all-start.2 = ((bf16[16,96,2048]{2,1,0:T(8,128)(2,1)}), bf16[16,96,2048]{2,1,0:T(8,128)(2,1)}, u32[]{:S(2)}, u32[]{:S(2)}) async-start(bf16[16,96,2048]{2,1,0:T(8,128)(2,1)} %bitcast.115), calls=%async_computation.4 | async-start | bytes 12582912 | tf_op jit(solution)/shard_map/all_to_all | solution.py:190
  392.9 142.4 %all-to-all-start.1 = ((bf16[16,96,2048]{2,1,0:T(8,128)(2,1)}), bf16[16,96,2048]{2,1,0:T(8,128)(2,1)}, u32[]{:S(2)}, u32[]{:S(2)}) async-start(bf16[16,96,2048]{2,1,0:T(8,128)(2,1)} %bitcast.117), calls=%async_computation.3 | async-start | bytes 12582912 | tf_op jit(solution)/shard_map/all_to_all | solution.py:188
  535.3 142.2 %all-to-all-start.3 = ((bf16[16,96,2048]{2,1,0:T(8,128)(2,1)}), bf16[16,96,2048]{2,1,0:T(8,128)(2,1)}, u32[]{:S(2)}, u32[]{:S(2)}) async-start(bf16[16,96,2048]{2,1,0:T(8,128)(2,1)} %bitcast.116), calls=%async_computation.5 | async-start | bytes 12582912 | tf_op jit(solution)/shard_map/all_to_all | solution.py:188
  540.0 35.0 %all-gather.2.cloned.1.call-start = ((), (), s32[]{:S(2)}) async-start(), calls=%async_computation.7 | async-start | bytes 3145728 | tf_op jit(solution)/shard_map/all_gather | solution.py:166
  540.8 162.0 %reduce-scatter.5.cloned.1.call-start = ((), (), s32[]{:S(2)}) async-start(), calls=%async_computation.8 | async-start | bytes 3145728 | tf_op jit(solution)/shard_map/reduce_scatter | solution.py:173
  577.6 5.9 copy-start.8
  689.9 7.6 %copy-start.2 = (bf16[1024,2048]{1,0:T(8,128)(2,1)S(1)}, bf16[1024,2048]{1,0:T(8,128)(2,1)}, u32[]{:S(2)}) copy-start(bf16[1024,2048]{1,0:T(8,128)(2,1)} %gather_fusion.1) | copy-start | bytes 12582916
  697.5 5.3 copy-start.4
Sparse Core Ops, SparseCore 0:
  55.5 32.7 reduce-scatter.2
  542.4 32.5 all-gather.1
  583.6 31.8 reduce-scatter.4
where the time goes:
time: 723 us; the launch traced here: 713 us
  waiting for transfers between devices  487 us (67%)
  local copies, waits for them, and re-layouts  65.2 us (9%)
  matrix products  59.3 us (8%)
  other arithmetic  47.8 us (7%)
  starting transfers between devices  39.8 us (6%)
  between operations  14.1 us (2%)
    all_to_all x2, waiting for transfers between devices, shards(): lax.all_to_all(packed, 'sp', split_axis=0, concat_axis=0, tiled=True)  232 us
    all_to_all x2, waiting for transfers between devices, shards(): lax.all_to_all(run_expert(lax.all_to_all(packed, 'sp', split_axis=0, conc...  198 us
    all_gather x1, waiting for transfers between devices, shards(): shard_rows = lax.all_gather(normed, 'tp', axis=0, tiled=True)  34.2 us
    gather x2, local copies, waits for them, and re-layouts, combine_rows(): returned.reshape(-1, returned.shape[-1])[slot_place]  25.1 us
    dot_general x2, matrix products, run_expert(): jnp.dot(hidden, down_w, preferred_element_type=jnp.float32)  23.5 us
    reduce_scatter x1, waiting for transfers between devices, shards(): lax.psum_scatter(jnp.dot(attended, w_out, preferred_element_type=jnp.floa...  22.8 us
    dot_general x2, matrix products, run_expert(): jnp.dot(flat_rows, gate_w, preferred_element_type=jnp.float32)  17.2 us
  transfers between devices with their start and end apart: 13, of which 6 were waited for; matrix products, arithmetic and copies ran while one was open for 19% of the time, Pallas kernels for 0%

commit v1 on v0

v1 whole, which is shorter than its diff:
```python
import math

import jax
import jax.numpy as jnp
from jax import lax
from jax.experimental import pallas as pl
from jax.experimental.pallas import tpu as pltpu
from jax.sharding import PartitionSpec as P

HD = 64
WINDOW = 128
PARTS = 2


norm_eps = 1e-06


def extended(cells, sides, width):
    for axis, dim in sides:
        count = lax.axis_size(axis)
        ends = count - 1
        head = lax.slice_in_dim(cells, 0, width, axis=dim)
        tail = lax.slice_in_dim(cells, cells.shape[dim] - width, cells.shape[dim], axis=dim)
        cells = jnp.concatenate(
            [
                lax.ppermute(tail, axis, [(i, (i + 1) % count) for i in range(ends)]),
                cells,
                lax.ppermute(head, axis, [((i + 1) % count, i) for i in range(ends)]),
            ],
            axis=dim,
        )
    return cells


def band_blocks(padded, width):
    span_count = padded.shape[0] // width - 2
    shaped = padded.reshape((span_count + 2, width) + padded.shape[1:])
    return jnp.concatenate(
        [
            shaped[0:span_count:2],
            shaped[1 : span_count + 1 : 2],
            shaped[2 : span_count + 2 : 2],
            shaped[3 : span_count + 3 : 2],
        ],
        axis=1,
    )


def attend(queries, ext_keys, ext_values, ext_marks, own_marks, sink_logit):
    tok_count = queries.shape[0]
    head_count = sink_logit.shape[0]
    key_heads = ext_keys.shape[1] // HD
    group_size = head_count // key_heads
    query_span = 2 * WINDOW
    block_count = tok_count // query_span
    query_blocks = queries.reshape(block_count, query_span, key_heads, group_size, HD)
    key_blocks = band_blocks(ext_keys, WINDOW).reshape(block_count, 4 * WINDOW, key_heads, HD)
    value_blocks = band_blocks(ext_values, WINDOW).reshape(block_count, 4 * WINDOW, key_heads, HD)
    mark_blocks = band_blocks(ext_marks, WINDOW)
    query_marks = own_marks.reshape(block_count, query_span)
    scores = jnp.einsum(
        "nqkgd,nmkd->nkgqm", query_blocks, key_blocks, preferred_element_type=jnp.float32
    ) * HD ** (-0.5)
    offset = (
        jnp.arange(query_span, dtype=jnp.int32)[:, None]
        - jnp.arange(4 * WINDOW, dtype=jnp.int32)[None, :]
        + WINDOW
    )
    allowed = (jnp.abs(offset) <= WINDOW)[None] & (
        mark_blocks[:, None, :] == query_marks[:, :, None]
    )
    scores = jnp.where(allowed[:, None, None], scores, -jnp.inf)
    sink_term = sink_logit.reshape(key_heads, group_size)[None, :, :, None, None]
    row_max = jnp.maximum(jnp.max(scores, axis=-1, keepdims=True), sink_term)
    exp_scores = jnp.exp(scores - row_max)
    attn_probs = (
        exp_scores / (jnp.sum(exp_scores, axis=-1, keepdims=True) + jnp.exp(sink_term - row_max))
    ).astype(jnp.bfloat16)
    result = jnp.einsum(
        "nkgqm,nmkd->nqkgd", attn_probs, value_blocks, preferred_element_type=jnp.float32
    )
    return result.astype(jnp.bfloat16).reshape(tok_count, head_count * HD)


def expert_kernel(rows_ref, scale_ref, gate_ref, up_ref, down_ref, side_ref, side_down_ref, out_ref):
    rows = rows_ref[...]
    gated = jnp.dot(rows, gate_ref[...], preferred_element_type=jnp.float32)
    lifted = jnp.dot(rows, up_ref[...], preferred_element_type=jnp.float32)
    hidden = (gated / (1.0 + jnp.exp(-gated)) * lifted).astype(jnp.bfloat16)
    produced = jnp.dot(hidden, down_ref[...], preferred_element_type=jnp.float32)
    side = jnp.dot(rows, side_ref[...], preferred_element_type=jnp.float32)
    width = side.shape[1] // 2
    side_gate, side_up = side[:, :width], side[:, width:]
    side_hidden = (side_gate / (1.0 + jnp.exp(-side_gate)) * side_up).astype(jnp.bfloat16)
    shared = jnp.dot(side_hidden, side_down_ref[...], preferred_element_type=jnp.float32)
    out_ref[...] = (
        scale_ref[...] * produced.astype(jnp.bfloat16).astype(jnp.float32) + shared
    ).astype(jnp.bfloat16)


def run_experts(rows, scale, gate_w, up_w, down_w, side_w, side_down):
    count, width = rows.shape
    tile = math.gcd(count, 256)
    whole = lambda w: pl.BlockSpec(w.shape, lambda i: (0, 0))
    units = gate_w.shape[1] + side_w.shape[1] // 2
    return pl.pallas_call(
        expert_kernel,
        grid=(count // tile,),
        in_specs=[
            pl.BlockSpec((tile, width), lambda i: (i, 0)),
            pl.BlockSpec((tile, 1), lambda i: (i, 0)),
            whole(gate_w),
            whole(up_w),
            whole(down_w),
            whole(side_w),
            whole(side_down),
        ],
        out_specs=pl.BlockSpec((tile, width), lambda i: (i, 0)),
        out_shape=jax.ShapeDtypeStruct((count, width), jnp.bfloat16),
        compiler_params=pltpu.CompilerParams(
            dimension_semantics=("arbitrary",), vmem_limit_bytes=48 * 1024 * 1024
        ),
        cost_estimate=pl.CostEstimate(
            flops=6 * count * width * units,
            bytes_accessed=4 * count * width + 6 * units * width,
            transcendentals=count * units,
        ),
    )(rows, scale, gate_w, up_w, down_w, side_w, side_down)


def shared_slice(shared_gate, shared_up, shared_down):
    sp_count, tp_count = lax.axis_size("sp"), lax.axis_size("tp")
    own, side = lax.axis_index("tp"), lax.axis_index("sp")
    units = shared_gate.shape[1] * tp_count // sp_count
    per_owner = sp_count // tp_count
    owner, offset = side // per_owner, (side % per_owner) * units
    held = jnp.concatenate(
        [
            lax.dynamic_slice_in_dim(shared_gate, offset, units, axis=1).T,
            lax.dynamic_slice_in_dim(shared_up, offset, units, axis=1).T,
            lax.dynamic_slice_in_dim(shared_down, offset, units, axis=0),
        ],
        axis=0,
    )
    chosen = held
    for shift in range(1, tp_count):
        came = lax.ppermute(held, "tp", [(i, (i + shift) % tp_count) for i in range(tp_count)])
        chosen = jnp.where((own - shift) % tp_count == owner, came, chosen)
    padded = -(-units // 128) * 128
    grown = [
        jnp.pad(chosen[i * units : (i + 1) * units], ((0, padded - units), (0, 0))) for i in range(3)
    ]
    return jnp.concatenate(grown[:2], axis=0).T, grown[2]


def shards(
    queries,
    keys,
    values,
    doc_ids,
    sink_logit,
    w_out,
    residual,
    ffn_gain,
    expert_ids,
    expert_weight,
    exp_gate,
    exp_up,
    exp_down,
    shared_gate,
    shared_up,
    shared_down,
):
    marks = (doc_ids + 1).astype(jnp.bfloat16)
    kv = keys.shape[1]
    joined = jnp.concatenate(
        [keys, values, jnp.broadcast_to(marks[:, None], (marks.shape[0], 128))], axis=1
    )
    extended_all = extended(joined, (("sp", 0),), WINDOW)
    ext_keys, ext_values, ext_marks = (
        extended_all[:, :kv],
        extended_all[:, kv : 2 * kv],
        extended_all[:, 2 * kv],
    )
    attended = attend(queries, ext_keys, ext_values, ext_marks, marks, sink_logit)
    row_count = residual.shape[0]
    mixed = lax.psum_scatter(
        jnp.dot(attended, w_out, preferred_element_type=jnp.float32).astype(jnp.bfloat16),
        "tp",
        scatter_dimension=0,
        tiled=True,
    ).astype(jnp.float32)
    resid = (residual.astype(jnp.float32) + mixed).astype(jnp.bfloat16)
    resid_f = resid.astype(jnp.float32)
    normed = (
        resid_f
        * lax.rsqrt(jnp.mean(resid_f * resid_f, axis=-1, keepdims=True) + norm_eps)
        * ffn_gain
    ).astype(jnp.bfloat16)
    side_w, side_down = shared_slice(shared_gate, shared_up, shared_down)
    sp_count = lax.axis_size("sp")
    chosen = expert_ids[:, :, None] == jnp.arange(sp_count, dtype=jnp.int32)
    table = jnp.sum(jnp.where(chosen, expert_weight[:, :, None], 0.0), axis=1)
    scales = lax.all_to_all(table.T, "sp", split_axis=0, concat_axis=0, tiled=True)
    part_rows = row_count // PARTS
    sums = []
    for part in range(PARTS):
        begin = part * part_rows
        gathered = lax.all_gather(normed[begin : begin + part_rows], "sp", axis=0, tiled=True)
        scale = scales[:, begin : begin + part_rows].reshape(-1, 1)
        produced = run_experts(
            gathered, scale, exp_gate[0], exp_up[0], exp_down[0], side_w, side_down
        )
        sums.append(lax.psum_scatter(produced, "sp", scatter_dimension=0, tiled=True))
    added = jnp.concatenate(sums, axis=0)
    return (resid.astype(jnp.float32) + added.astype(jnp.float32)).astype(jnp.bfloat16)


def solution(mesh):
    placed = (
        P("sp", "tp"),
        P("sp", "tp"),
        P("sp", "tp"),
        P("sp"),
        P("tp"),
        P("tp", None),
        P(("sp", "tp"), None),
        P(),
        P(("sp", "tp"), None),
        P(("sp", "tp"), None),
        P("sp", None, None),
        P("sp", None, None),
        P("sp", None, None),
        P(None, "tp"),
        P(None, "tp"),
        P("tp", None),
    )
    return jax.shard_map(
        shards, mesh=mesh, in_specs=placed, out_specs=P(("sp", "tp"), None), check_vma=False
    )
```

time: 723 us -> 455 us (0.63); the launches traced: 713 us -> 453 us
  waiting for transfers between devices: 487 us -> 325 us
  Pallas kernels: 0 us -> 56.1 us
  matrix products: 59.3 us -> 10.1 us
  local copies, waits for them, and re-layouts: 65.2 us -> 22.1 us
  other arithmetic: 47.8 us -> 12.9 us
  starting transfers between devices: 39.8 us -> 13.1 us
    all_to_all x4 -> x1, waiting for transfers between devices: 430 us -> 4.1 us  [shards(): lax.all_to_all(table.T, 'sp', split_axis=0, concat_axis=0, tiled=True)]
    reduce_scatter x1 -> x2, waiting for transfers between devices: 0.01 us -> 184 us  [shards(): lax.psum_scatter(produced, 'sp', scatter_dimension=0, tiled=True)]
    all_gather x1 -> x2, waiting for transfers between devices: 34.2 us -> 102 us  [shards(): lax.all_gather(normed[begin:begin + part_rows], 'sp', axis=0, tiled=True)]
    pallas_call x0 -> x2, Pallas kernels: none -> 56.1 us  [run_experts(): pl.pallas_call(expert_kernel, grid=(count // tile,), in_specs=[pl.BlockSp...]
    dot_general x6 -> x0, matrix products: 49.1 us -> none  [the longest x2 23.5 us: run_expert(): jnp.dot(hidden, down_w, preferred_element_type=jnp.float32)]
    gather x4 -> x0, local copies, waits for them, and re-layouts: 39.4 us -> none  [the longest x2 25.1 us: combine_rows(): returned.reshape(-1, returned.shape[-1])[slot_place]]
    all_to_all x4 -> x1, starting transfers between devices: 21.2 us -> 6.77 us  [shards(): lax.all_to_all(table.T, 'sp', split_axis=0, concat_axis=0, tiled=True)]
    reduce_sum x4 -> x1, other arithmetic: 12.9 us -> 0.02 us  [shards(): table = jnp.sum(jnp.where(chosen, expert_weight[:, :, None], 0.0), axis=1)]
  transfers between devices with their start and end apart: 13 -> 9, of which waited for: 6 -> 7; matrix products, arithmetic and copies ran while one was open for 19% -> 2% of each run, Pallas kernels for 0% -> 12%
where the time goes in v1:
time: 455 us; the launch traced here: 453 us
  waiting for transfers between devices  325 us (71%)
  Pallas kernels  56.1 us (12%)
  local copies, waits for them, and re-layouts  22.1 us (5%)
  between operations  13.5 us (3%)
  starting transfers between devices  13.1 us (3%)
  other arithmetic  12.9 us (3%)
  matrix products  10.1 us (2%)
    reduce_scatter x2, waiting for transfers between devices, shards(): lax.psum_scatter(produced, 'sp', scatter_dimension=0, tiled=True)  184 us
    all_gather x2, waiting for transfers between devices, shards(): lax.all_gather(normed[begin:begin + part_rows], 'sp', axis=0, tiled=True)  102 us
    pallas_call x2, Pallas kernels, run_experts(): pl.pallas_call(expert_kernel, grid=(count // tile,), in_specs=[pl.BlockSp...  56.1 us
    reduce_scatter x1, waiting for transfers between devices, shards(): lax.psum_scatter(jnp.dot(attended, w_out, preferred_element_type=jnp.floa...  31.4 us
    unnamed x42, local copies, waits for them, and re-layouts  11 us
  transfers between devices with their start and end apart: 9, of which 7 were waited for; matrix products, arithmetic and copies ran while one was open for 2% of the time, Pallas kernels for 12%

profile of v1, /device:TPU:13, one launch (start us, length us, event | category | flops | bytes accessed | tf_op | source)
XLA Modules:
  0.0 453.0 jit_solution(13340162137230098640)
XLA Ops:
  6.5 0.9 add_convert_fusion.1
  7.5 1.5 pad_maximum_fusion.6
  9.1 3.7 collective-permute-start
  12.8 1.9 collective-permute-start.1
  14.7 2.2 reshape.84
  17.1 2.8 collective-permute-done.1
  19.9 1.1 pad_maximum_fusion
  21.0 0.7 fusion.18
  21.9 0.6 slice.82
  22.5 0.6 slice.83
  23.1 0.7 fusion.20
  23.8 1.6 copy.102
  25.3 1.6 copy.103
  26.9 1.6 copy.104
  28.5 0.8 copy.105
  29.2 0.7 pad_maximum_fusion.7
  29.9 0.3 compare_and_fusion
  30.2 1.0 pad_maximum_fusion.3
  31.1 1.8 fusion.1
  33.0 1.8 fusion
  34.8 1.4 copy-done.4
  36.9 5.7 %fusion.10 = bf16[2,256,2,4,64]{1,4,3,2,0:T(8,128)(2,1)S(1)} fusion(bf16[2,512,2,64,1]{1,3,4,2,0:T(8,128)(2,1)S(1)} %bitcast.63, f32[2,2,512,256,4]{3,2,4,1,0:T(8,128)} %copy-done.4, f32[2,2,4,256]{3,2,1,0:T(4,128)S(1)} %exponential_add_fusion, f32[2,2,4,256]{3,2,1,0:T(4,128)S(1)} %broadcast_maximum_fusion, pred[2,256,512]{1,2,0:T(8,128)(4,1)S(1)} %compare_and_fusion), kind=kOutput, calls=%fused_computation.20 | convolution fusion | flops 279183360 | bytes 9469952 | tf_op jit(solution)/shard_map/nkgqm,nmkd->nqkgd/dot_general | solution.py:79
  42.5 0.5 copy.84
  43.2 2.6 convolution_convert_fusion
  45.9 31.4 %reduce-scatter.4.cloned.1.call-done = bf16[256,2048]{1,0:T(8,128)(2,1)} async-done(((bf16[512,2048]{1,0:T(8,128)(2,1)}), bf16[256,2048]{1,0:T(8,128)(2,1)}) %reduce-scatter.4.cloned.1.call-update) | async-done | bytes 1048592 | tf_op jit(solution)/shard_map/reduce_scatter | solution.py:187
  77.3 1.7 fusion.3
  79.1 0.5 fusion.5
  79.6 1.1 fusion.17
  80.7 0.7 all-gather.5.cloned.1.call-update
  81.4 1.4 constant_dynamic-slice_fusion.1
  83.2 0.9 constant_dynamic-slice_fusion
  84.2 0.3 collective-permute-start.2
  84.6 0.6 copy.85
  85.2 6.8 %all-to-all-start = ((f32[16,1,256]{2,1,0:T(1,128)}), f32[16,1,256]{2,1,0:T(1,128)S(1)}, u32[]{:S(2)}, u32[]{:S(2)}) async-start(f32[16,1,256]{2,1,0:T(1,128)} %copy.85), calls=%async_computation.1 | async-start | bytes 32768 | tf_op jit(solution)/shard_map/all_to_all | solution.py:204
  92.0 0.2 reduce-scatter.6.cloned.1.call-start
  92.2 4.1 all-to-all-done
  96.3 0.4 copy.88.scale_ref
  97.0 0.5 copy.89.side_ref
  97.5 57.3 %all-gather.3.cloned.1.call-done.rows_ref = bf16[2048,2048]{1,0:T(8,128)(2,1)} async-done(((bf16[128,2048]{1,0:T(8,128)(2,1)}), bf16[2048,2048]{1,0:T(8,128)(2,1)}) %all-gather.3.cloned.1.call-update) | async-done | bytes 8388624 | tf_op jit(solution)/shard_map/all_gather | solution.py:209
  154.8 1.6 copy-done.2
  156.4 28.0 %shard_map.154 = bf16[2048,2048]{1,0:T(8,128)(2,1)} custom-call(bf16[2048,2048]{1,0:T(8,128)(2,1)} %all-gather.3.cloned.1.call-done.rows_ref, f32[2048,1]{1,0:T(8,128)S(1)} %copy.88.scale_ref, bf16[2048,512]{1,0:T(8,128)(2,1)S(1)} %bitcast.52, bf16[2048,512]{1,0:T(8,128)(2,1)} %bitcast.72, bf16[512,2048]{1,0:T(8,128)(2,1)} %bitcast.74, ...), custom_call_target="tpu_custom_call" | custom-call | flops 16106127360 | bytes 24641536 | tf_op jit(solution)/shard_map/pallas_call | solution.py:106
  184.5 0.4 copy.90.scale_ref
  184.8 45.0 %all-gather.5.cloned.1.call-done.rows_ref = bf16[2048,2048]{1,0:T(8,128)(2,1)} async-done(((bf16[128,2048]{1,0:T(8,128)(2,1)}), bf16[2048,2048]{1,0:T(8,128)(2,1)}) %all-gather.5.cloned.1.call-update) | async-done | bytes 8388624 | tf_op jit(solution)/shard_map/all_gather | solution.py:209
  229.9 1.6 copy-done.3
  231.5 28.1 %shard_map.155 = bf16[2048,2048]{1,0:T(8,128)(2,1)} custom-call(bf16[2048,2048]{1,0:T(8,128)(2,1)} %all-gather.5.cloned.1.call-done.rows_ref, f32[2048,1]{1,0:T(8,128)S(1)} %copy.90.scale_ref, bf16[2048,512]{1,0:T(8,128)(2,1)S(1)} %bitcast.53, bf16[2048,512]{1,0:T(8,128)(2,1)} %bitcast.73, bf16[512,2048]{1,0:T(8,128)(2,1)} %bitcast.75, ...), custom_call_target="tpu_custom_call" | custom-call | flops 16106127360 | bytes 24641536 | tf_op jit(solution)/shard_map/pallas_call | solution.py:106
  259.6 76.8 %reduce-scatter.6.cloned.1.call-done = bf16[128,2048]{1,0:T(8,128)(2,1)} async-done(((bf16[2048,2048]{1,0:T(8,128)(2,1)}), bf16[128,2048]{1,0:T(8,128)(2,1)}) %reduce-scatter.6.cloned.1.call-update) | async-done | bytes 524304 | tf_op jit(solution)/shard_map/reduce_scatter | solution.py:214
  336.4 107.0 %reduce-scatter.8.cloned.1.call-done = bf16[128,2048]{1,0:T(8,128)(2,1)} async-done(((bf16[2048,2048]{1,0:T(8,128)(2,1)}), bf16[128,2048]{1,0:T(8,128)(2,1)}) %reduce-scatter.8.cloned.1.call-update) | async-done | bytes 524304 | tf_op jit(solution)/shard_map/reduce_scatter | solution.py:214
  443.4 3.1 fusion.6
  (64 shorter events, 2.3 us)
Async XLA Ops:
  6.5 36.6 %copy-start = (bf16[512,2048]{1,0:T(8,128)(2,1)S(1)}, bf16[512,2048]{1,0:T(8,128)(2,1)}, u32[]{:S(2)}) copy-start(bf16[512,2048]{1,0:T(8,128)(2,1)} %param.21) | copy-start | bytes 6291460
  6.5 13.4 %copy-start.9 = (bf16[512,128]{1,0:T(8,128)(2,1)S(1)}, bf16[512,128]{1,0:T(8,128)(2,1)}, u32[]{:S(2)}) copy-start(bf16[512,128]{1,0:T(8,128)(2,1)} %param.18) | copy-start | bytes 393220
  6.5 10.4 %copy-start.14 = (f32[8]{0:T(128)S(1)}, f32[8]{0:T(128)}, u32[]{:S(2)}) copy-start(f32[8]{0:T(128)} %param.20) | copy-start | bytes 100
  6.5 70.8 %reduce-scatter.4.cloned.1.call-start = ((), (), s32[]{:S(2)}) async-start(), calls=%async_computation.4 | async-start | bytes 3145728 | tf_op jit(solution)/shard_map/reduce_scatter | solution.py:187
  9.1 8.1 %collective-permute-start = (bf16[128,384]{1,0:T(8,128)(2,1)}, bf16[128,384]{1,0:T(8,128)(2,1)}, u32[]{:S(2)}, u32[]{:S(2)}) collective-permute-start(bf16[128,384]{1,0:T(8,128)(2,1)} %get-tuple-element.12), channel_id=1, source_target_pairs={{0,2},{2,4},{4,6},{6,8},{8,10},{10,12},{12,14},{14,16},{16,18},{18... | collective-permute-start | bytes 294920 | tf_op jit(solution)/shard_map/ppermute | solution.py:26
  12.8 7.2 %collective-permute-start.1 = (bf16[128,384]{1,0:T(8,128)(2,1)}, bf16[128,384]{1,0:T(8,128)(2,1)}, u32[]{:S(2)}, u32[]{:S(2)}) collective-permute-start(bf16[128,384]{1,0:T(8,128)(2,1)} %get-tuple-element.13), channel_id=1, source_target_pairs={{2,0},{4,2},{6,4},{8,6},{10,8},{12,10},{14,12},{16,14},{18,16},{20... | collective-permute-start | bytes 294920 | tf_op jit(solution)/shard_map/ppermute | solution.py:28
  32.9 3.2 copy-start.4
  33.0 3.2 copy-start.8
  45.8 31.5 %copy-start.5 = (bf16[256,2048]{1,0:T(8,128)(2,1)S(1)}, bf16[256,2048]{1,0:T(8,128)(2,1)}, u32[]{:S(2)}) copy-start(bf16[256,2048]{1,0:T(8,128)(2,1)} %param.22) | copy-start | bytes 3145732
  45.8 33.3 %copy-start.11 = (f32[2048]{0:T(1024)S(1)}, f32[2048]{0:T(1024)}, u32[]{:S(2)}) copy-start(f32[2048]{0:T(1024)} %param.23) | copy-start | bytes 24580
  45.8 109.0 %all-gather.3.cloned.1.call-start = ((), (), s32[]{:S(2)}) async-start(), calls=%async_computation.5 | async-start | bytes 8912896 | tf_op jit(solution)/shard_map/all_gather | solution.py:209
  77.3 1.8 copy-start.7
  79.6 1.9 copy-start.10
  80.7 149.2 %all-gather.5.cloned.1.call-start = ((), (), s32[]{:S(2)}) async-start(), calls=%async_computation.7 | async-start | bytes 8912896 | tf_op jit(solution)/shard_map/all_gather | solution.py:209
  81.4 3.1 copy-start.12
  81.4 3.1 copy-start.13
  84.2 12.5 %collective-permute-start.2 = (bf16[96,2048]{1,0:T(8,128)(2,1)S(1)}, bf16[96,2048]{1,0:T(8,128)(2,1)S(1)}, u32[]{:S(2)}, u32[]{:S(2)}) collective-permute-start(bf16[96,2048]{1,0:T(8,128)(2,1)S(1)} %pad_maximum_fusion.1), channel_id=1, source_target_pairs={{0,1},{1,0},{2,3},{3,2},{4,5},{5,4},{6,7},{7,6},{8,9},{9,8},{10,11... | collective-permute-start | bytes 1179656 | tf_op jit(solution)/shard_map/ppermute | solution.py:147
  85.2 11.1 %all-to-all-start = ((f32[16,1,256]{2,1,0:T(1,128)}), f32[16,1,256]{2,1,0:T(1,128)S(1)}, u32[]{:S(2)}, u32[]{:S(2)}) async-start(f32[16,1,256]{2,1,0:T(1,128)} %copy.85), calls=%async_computation.1 | async-start | bytes 32768 | tf_op jit(solution)/shard_map/all_to_all | solution.py:204
  92.0 244.5 %reduce-scatter.6.cloned.1.call-start = ((), (), s32[]{:S(2)}) async-start(), calls=%async_computation.6 | async-start | bytes 8912896 | tf_op jit(solution)/shard_map/reduce_scatter | solution.py:214
  154.8 1.6 copy-start.2
  184.4 259.0 %reduce-scatter.8.cloned.1.call-start = ((), (), s32[]{:S(2)}) async-start(), calls=%async_computation.8 | async-start | bytes 8912896 | tf_op jit(solution)/shard_map/reduce_scatter | solution.py:214
  229.9 1.6 copy-start.3
  259.5 183.9 %copy-start.6 = (bf16[256,2048]{1,0:T(8,128)(2,1)S(1)}, bf16[256,2048]{1,0:T(8,128)(2,1)}, u32[]{:S(2)}) copy-start(bf16[256,2048]{1,0:T(8,128)(2,1)} %param.22) | copy-start | bytes 3145732
  259.6 186.9 %copy-start.1 = (bf16[512,2048]{1,0:T(8,128)(2,1)S(1)}, bf16[512,2048]{1,0:T(8,128)(2,1)}, u32[]{:S(2)}) copy-start(bf16[512,2048]{1,0:T(8,128)(2,1)} %param.21) | copy-start | bytes 6291460
Sparse Core Ops, SparseCore 0:
  45.9 31.3 reduce-scatter.3
  80.8 73.9 all-gather.2
  157.0 72.8 all-gather.4
  233.8 102.5 reduce-scatter.5
  340.3 103.0 reduce-scatter.7

commit v2 on v1

--- a/solution.py
+++ b/solution.py
@@ -9,7 +9,8 @@
 
 HD = 64
 WINDOW = 128
-PARTS = 2
+PARTS = 4
+DIRECT = 2
 
 
 norm_eps = 1e-06
@@ -153,6 +154,19 @@
     return jnp.concatenate(grown[:2], axis=0).T, grown[2]
 
 
+def tp_scatter(product, row_count):
+    count, own = lax.axis_size("tp"), lax.axis_index("tp")
+    total = lax.dynamic_slice_in_dim(product, own * row_count, row_count, axis=0)
+    for shift in range(1, count):
+        target = (own + shift) % count
+        block = lax.dynamic_slice_in_dim(product, target * row_count, row_count, axis=0)
+        came = lax.ppermute(
+            block.astype(jnp.bfloat16), "tp", [(i, (i + shift) % count) for i in range(count)]
+        )
+        total = total + came.astype(jnp.float32)
+    return total
+
+
 def shards(
     queries,
     keys,
@@ -184,12 +198,7 @@
     )
     attended = attend(queries, ext_keys, ext_values, ext_marks, marks, sink_logit)
     row_count = residual.shape[0]
-    mixed = lax.psum_scatter(
-        jnp.dot(attended, w_out, preferred_element_type=jnp.float32).astype(jnp.bfloat16),
-        "tp",
-        scatter_dimension=0,
-        tiled=True,
-    ).astype(jnp.float32)
+    mixed = tp_scatter(jnp.dot(attended, w_out, preferred_element_type=jnp.float32), row_count)
     resid = (residual.astype(jnp.float32) + mixed).astype(jnp.bfloat16)
     resid_f = resid.astype(jnp.float32)
     normed = (
@@ -211,9 +220,15 @@
         produced = run_experts(
             gathered, scale, exp_gate[0], exp_up[0], exp_down[0], side_w, side_down
         )
-        sums.append(lax.psum_scatter(produced, "sp", scatter_dimension=0, tiled=True))
+        if part < DIRECT:
+            came = lax.all_to_all(produced, "sp", split_axis=0, concat_axis=0, tiled=True)
+            came = came.reshape(sp_count, part_rows, came.shape[1])
+            sums.append(jnp.sum(came.astype(jnp.float32), axis=0))
+        else:
+            summed = lax.psum_scatter(produced, "sp", scatter_dimension=0, tiled=True)
+            sums.append(summed.astype(jnp.float32))
     added = jnp.concatenate(sums, axis=0)
-    return (resid.astype(jnp.float32) + added.astype(jnp.float32)).astype(jnp.bfloat16)
+    return (resid.astype(jnp.float32) + added).astype(jnp.bfloat16)
 
 
 def solution(mesh):

time: 455 us -> 546 us (1.20)
  waiting for transfers between devices: 325 us -> 374 us
  starting transfers between devices: 13.1 us -> 28.7 us
  other arithmetic: 12.9 us -> 23.3 us
  local copies, waits for them, and re-layouts: 22.1 us -> 29.5 us
  Pallas kernels: 56.1 us -> 63.2 us
    all_gather x2 -> x4, waiting for transfers between devices: 102 us -> 203 us  [shards(): lax.all_gather(normed[begin:begin + part_rows], 'sp', axis=0, tiled=True)]
    reduce_scatter x3 -> x2, waiting for transfers between devices: 215 us -> 140 us  [shards(): summed = lax.psum_scatter(produced, 'sp', scatter_dimension=0, tiled=True)]
    ppermute x0 -> x1, waiting for transfers between devices: none -> 22.1 us  [tp_scatter(): lax.ppermute(block.astype(jnp.bfloat16), 'tp', [(i, (i + shift) % count)...]
    all_to_all x0 -> x2, starting transfers between devices: none -> 13.5 us  [shards(): lax.all_to_all(produced, 'sp', split_axis=0, concat_axis=0, tiled=True)]
    pallas_call x2 -> x4, Pallas kernels: 56.1 us -> 63.2 us  [run_experts(): pl.pallas_call(expert_kernel, grid=(count // tile,), in_specs=[pl.BlockSp...]
    reduce_sum x0 -> x2, other arithmetic: none -> 6.99 us  [shards(): sums.append(jnp.sum(came.astype(jnp.float32), axis=0))]
    unnamed x42 -> x50, local copies, waits for them, and re-layouts: 11 us -> 16.2 us
  transfers between devices with their start and end apart: 9 -> 13, of which waited for: 7 -> 9; matrix products, arithmetic and copies ran while one was open for 2% -> 3% of each run, Pallas kernels for 12% -> 12%
where the time goes in v2:
time: 546 us; the launch traced here: 541 us
  waiting for transfers between devices  374 us (68%)
  Pallas kernels  63.2 us (12%)
  local copies, waits for them, and re-layouts  29.5 us (5%)
  starting transfers between devices  28.7 us (5%)
  other arithmetic  23.3 us (4%)
  between operations  13.9 us (3%)
  matrix products  8.77 us (2%)
    all_gather x4, waiting for transfers between devices, shards(): lax.all_gather(normed[begin:begin + part_rows], 'sp', axis=0, tiled=True)  203 us
    reduce_scatter x2, waiting for transfers between devices, shards(): summed = lax.psum_scatter(produced, 'sp', scatter_dimension=0, tiled=True)  140 us
    pallas_call x4, Pallas kernels, run_experts(): pl.pallas_call(expert_kernel, grid=(count // tile,), in_specs=[pl.BlockSp...  63.2 us
    ppermute x1, waiting for transfers between devices, tp_scatter(): lax.ppermute(block.astype(jnp.bfloat16), 'tp', [(i, (i + shift) % count)...  22.1 us
    unnamed x50, local copies, waits for them, and re-layouts  16.2 us
    all_to_all x2, starting transfers between devices, shards(): lax.all_to_all(produced, 'sp', split_axis=0, concat_axis=0, tiled=True)  13.5 us
  transfers between devices with their start and end apart: 13, of which 9 were waited for; matrix products, arithmetic and copies ran while one was open for 3% of the time, Pallas kernels for 12%

profile of v2, /device:TPU:13, one launch (start us, length us, event | category | flops | bytes accessed | tf_op | source)
XLA Modules:
  0.0 541.5 jit_solution(16824259417530415535)
XLA Ops:
  7.5 1.5 pad_maximum_fusion.6
  9.1 3.7 collective-permute-start
  12.8 1.9 collective-permute-start.1
  14.7 2.2 reshape.100
  17.1 2.8 collective-permute-done.1
  19.9 1.1 pad_maximum_fusion
  23.7 1.6 copy.116
  25.3 1.6 copy.117
  26.8 1.6 copy.118
  30.1 1.0 pad_maximum_fusion.3
  31.0 1.8 fusion.1
  32.9 1.8 fusion
  34.7 1.4 copy-done.6
  36.8 5.7 %fusion.10 = bf16[2,256,2,4,64]{1,4,3,2,0:T(8,128)(2,1)S(1)} fusion(bf16[2,512,2,64,1]{1,3,4,2,0:T(8,128)(2,1)S(1)} %bitcast.67, f32[2,2,512,256,4]{3,2,4,1,0:T(8,128)} %copy-done.6, f32[2,2,4,256]{3,2,1,0:T(4,128)S(1)} %exponential_add_fusion, f32[2,2,4,256]{3,2,1,0:T(4,128)S(1)} %broadcast_maximum_fusion, pred[2,256,512]{1,2,0:T(8,128)(4,1)S(1)} %compare_and_fusion), kind=kOutput, calls=%fused_computation.22 | convolution fusion | flops 279183360 | bytes 9469952 | tf_op jit(solution)/shard_map/nkgqm,nmkd->nqkgd/dot_general | solution.py:80
  43.1 1.3 fusion.23
  44.5 1.9 copy-done.7
  46.6 1.3 collective-permute-start.2
  47.8 22.1 %collective-permute-done.2 = bf16[256,2048]{1,0:T(8,128)(2,1)} collective-permute-done((bf16[256,2048]{1,0:T(8,128)(2,1)S(1)}, bf16[256,2048]{1,0:T(8,128)(2,1)}, u32[]{:S(2)}, u32[]{:S(2)}) %collective-permute-start.2) | collective-permute-done | bytes 1048608 | tf_op jit(solution)/shard_map/ppermute | solution.py:163
  70.0 2.5 fusion.3
  72.8 1.0 fusion.17
  76.0 1.4 constant_dynamic-slice_fusion.1
  77.8 0.9 constant_dynamic-slice_fusion
  78.7 1.3 collective-permute-start.3
  80.6 6.6 %all-to-all-start = ((f32[16,1,256]{2,1,0:T(1,128)}), f32[16,1,256]{2,1,0:T(1,128)S(1)}, u32[]{:S(2)}, u32[]{:S(2)}) async-start(f32[16,1,256]{2,1,0:T(1,128)} %copy.95), calls=%async_computation | async-start | bytes 32768 | tf_op jit(solution)/shard_map/all_to_all | solution.py:213
  87.2 4.5 all-to-all-done
  92.5 1.1 fusion.12
  93.5 1.5 copy.99.side_ref
  95.1 30.1 %all-gather.5.cloned.1.call-done.rows_ref = bf16[1024,2048]{1,0:T(8,128)(2,1)} async-done(((bf16[64,2048]{1,0:T(8,128)(2,1)}), bf16[1024,2048]{1,0:T(8,128)(2,1)}) %all-gather.5.cloned.1.call-update) | async-done | bytes 4194320 | tf_op jit(solution)/shard_map/all_gather | solution.py:218
  125.1 1.6 copy-done.2
  126.7 15.9 %shard_map.154 = bf16[1024,2048]{1,0:T(8,128)(2,1)} custom-call(bf16[1024,2048]{1,0:T(8,128)(2,1)} %all-gather.5.cloned.1.call-done.rows_ref, f32[1024,1]{1,0:T(8,128)S(1)} %reshape.101.scale_ref, bf16[2048,512]{1,0:T(8,128)(2,1)S(1)} %bitcast.52, bf16[2048,512]{1,0:T(8,128)(2,1)} %bitcast.74, bf16[512,2048]{1,0:T(8,128)(2,1)} %bitcast.78, ...), custom_call_target="tpu_custom_call" | custom-call | flops 8053063680 | bytes 16252928 | tf_op jit(solution)/shard_map/pallas_call | solution.py:107
  142.6 5.6 %all-to-all-start.1 = ((bf16[16,64,2048]{2,1,0:T(8,128)(2,1)}), bf16[16,64,2048]{2,1,0:T(8,128)(2,1)}, u32[]{:S(2)}, u32[]{:S(2)}) async-start(bf16[16,64,2048]{2,1,0:T(8,128)(2,1)} %bitcast.57), calls=%async_computation.1 | async-start | bytes 8388608 | tf_op jit(solution)/shard_map/all_to_all | solution.py:224
  148.7 60.3 %all-gather.9.cloned.1.call-done.rows_ref = bf16[1024,2048]{1,0:T(8,128)(2,1)} async-done(((bf16[64,2048]{1,0:T(8,128)(2,1)}), bf16[1024,2048]{1,0:T(8,128)(2,1)}) %all-gather.9.cloned.1.call-update) | async-done | bytes 4194320 | tf_op jit(solution)/shard_map/all_gather | solution.py:218
  209.0 1.6 copy-done.3
  210.6 15.7 %shard_map.156 = bf16[1024,2048]{1,0:T(8,128)(2,1)} custom-call(bf16[1024,2048]{1,0:T(8,128)(2,1)} %all-gather.9.cloned.1.call-done.rows_ref, f32[1024,1]{1,0:T(8,128)S(1)} %reshape.103.scale_ref, bf16[2048,512]{1,0:T(8,128)(2,1)S(1)} %bitcast.53, bf16[2048,512]{1,0:T(8,128)(2,1)} %bitcast.75, bf16[512,2048]{1,0:T(8,128)(2,1)} %bitcast.79, ...), custom_call_target="tpu_custom_call" | custom-call | flops 8053063680 | bytes 16252928 | tf_op jit(solution)/shard_map/pallas_call | solution.py:107
  226.8 52.5 %all-gather.7.cloned.1.call-done.rows_ref = bf16[1024,2048]{1,0:T(8,128)(2,1)} async-done(((bf16[64,2048]{1,0:T(8,128)(2,1)}), bf16[1024,2048]{1,0:T(8,128)(2,1)}) %all-gather.7.cloned.1.call-update) | async-done | bytes 4194320 | tf_op jit(solution)/shard_map/all_gather | solution.py:218
  279.4 1.6 copy-done.4
  280.9 15.8 %shard_map.155 = bf16[1024,2048]{1,0:T(8,128)(2,1)} custom-call(bf16[1024,2048]{1,0:T(8,128)(2,1)} %all-gather.7.cloned.1.call-done.rows_ref, f32[1024,1]{1,0:T(8,128)S(1)} %reshape.102.scale_ref, bf16[2048,512]{1,0:T(8,128)(2,1)S(1)} %bitcast.54, bf16[2048,512]{1,0:T(8,128)(2,1)} %bitcast.76, bf16[512,2048]{1,0:T(8,128)(2,1)} %bitcast.80, ...), custom_call_target="tpu_custom_call" | custom-call | flops 8053063680 | bytes 16252928 | tf_op jit(solution)/shard_map/pallas_call | solution.py:107
  296.7 7.9 %all-to-all-start.2 = ((bf16[16,64,2048]{2,1,0:T(8,128)(2,1)}), bf16[16,64,2048]{2,1,0:T(8,128)(2,1)}, u32[]{:S(2)}, u32[]{:S(2)}) async-start(bf16[16,64,2048]{2,1,0:T(8,128)(2,1)} %bitcast.56), calls=%async_computation.2 | async-start | bytes 8388608 | tf_op jit(solution)/shard_map/all_to_all | solution.py:224
  305.4 60.1 %all-gather.11.cloned.1.call-done.rows_ref = bf16[1024,2048]{1,0:T(8,128)(2,1)} async-done(((bf16[64,2048]{1,0:T(8,128)(2,1)}), bf16[1024,2048]{1,0:T(8,128)(2,1)}) %all-gather.11.cloned.1.call-update) | async-done | bytes 4194320 | tf_op jit(solution)/shard_map/all_gather | solution.py:218
  365.5 1.6 copy-done.5
  367.1 15.9 %shard_map.157 = bf16[1024,2048]{1,0:T(8,128)(2,1)} custom-call(bf16[1024,2048]{1,0:T(8,128)(2,1)} %all-gather.11.cloned.1.call-done.rows_ref, f32[1024,1]{1,0:T(8,128)S(1)} %reshape.104.scale_ref, bf16[2048,512]{1,0:T(8,128)(2,1)S(1)} %bitcast.55, bf16[2048,512]{1,0:T(8,128)(2,1)} %bitcast.77, bf16[512,2048]{1,0:T(8,128)(2,1)} %bitcast.81, ...), custom_call_target="tpu_custom_call" | custom-call | flops 8053063680 | bytes 16252928 | tf_op jit(solution)/shard_map/pallas_call | solution.py:107
  383.0 66.0 %reduce-scatter.3.cloned.1.call-done = bf16[64,2048]{1,0:T(8,128)(2,1)} async-done(((bf16[1024,2048]{1,0:T(8,128)(2,1)}), bf16[64,2048]{1,0:T(8,128)(2,1)}) %reduce-scatter.3.cloned.1.call-update) | async-done | bytes 262160 | tf_op jit(solution)/shard_map/reduce_scatter | solution.py:228
  448.9 1.8 convert_element_type.62
  450.7 73.8 %reduce-scatter.5.cloned.1.call-done = bf16[64,2048]{1,0:T(8,128)(2,1)} async-done(((bf16[1024,2048]{1,0:T(8,128)(2,1)}), bf16[64,2048]{1,0:T(8,128)(2,1)}) %reduce-scatter.5.cloned.1.call-update) | async-done | bytes 262160 | tf_op jit(solution)/shard_map/reduce_scatter | solution.py:228
  524.5 1.8 convert_element_type.63
  526.3 3.8 convert_reduce_fusion.1
  530.2 3.2 convert_reduce_fusion
  533.4 1.3 fusion.6
  (90 shorter events, 13.0 us)
Async XLA Ops:
  6.5 36.6 %copy-start = (bf16[512,2048]{1,0:T(8,128)(2,1)S(1)}, bf16[512,2048]{1,0:T(8,128)(2,1)}, u32[]{:S(2)}) copy-start(bf16[512,2048]{1,0:T(8,128)(2,1)} %param.21) | copy-start | bytes 6291460
  6.5 13.4 %copy-start.13 = (bf16[512,128]{1,0:T(8,128)(2,1)S(1)}, bf16[512,128]{1,0:T(8,128)(2,1)}, u32[]{:S(2)}) copy-start(bf16[512,128]{1,0:T(8,128)(2,1)} %param.18) | copy-start | bytes 393220
  6.5 10.4 %copy-start.18 = (f32[8]{0:T(128)S(1)}, f32[8]{0:T(128)}, u32[]{:S(2)}) copy-start(f32[8]{0:T(128)} %param.20) | copy-start | bytes 100
  6.5 118.6 %all-gather.5.cloned.1.call-start = ((), (), s32[]{:S(2)}) async-start(), calls=%async_computation.5 | async-start | bytes 4456448 | tf_op jit(solution)/shard_map/all_gather | solution.py:218
  9.1 8.1 %collective-permute-start = (bf16[128,384]{1,0:T(8,128)(2,1)}, bf16[128,384]{1,0:T(8,128)(2,1)}, u32[]{:S(2)}, u32[]{:S(2)}) collective-permute-start(bf16[128,384]{1,0:T(8,128)(2,1)} %get-tuple-element.16), channel_id=1, source_target_pairs={{0,2},{2,4},{4,6},{6,8},{8,10},{10,12},{12,14},{14,16},{16,18},{18... | collective-permute-start | bytes 294920 | tf_op jit(solution)/shard_map/ppermute | solution.py:27
  12.8 7.2 %collective-permute-start.1 = (bf16[128,384]{1,0:T(8,128)(2,1)}, bf16[128,384]{1,0:T(8,128)(2,1)}, u32[]{:S(2)}, u32[]{:S(2)}) collective-permute-start(bf16[128,384]{1,0:T(8,128)(2,1)} %get-tuple-element.17), channel_id=1, source_target_pairs={{2,0},{4,2},{6,4},{8,6},{10,8},{12,10},{14,12},{16,14},{18,16},{20... | collective-permute-start | bytes 294920 | tf_op jit(solution)/shard_map/ppermute | solution.py:29
  32.8 3.3 copy-start.6
  32.9 3.3 copy-start.11
  44.4 2.0 copy-start.7
  46.4 23.6 %copy-start.12 = (bf16[256,2048]{1,0:T(8,128)(2,1)S(1)}, bf16[256,2048]{1,0:T(8,128)(2,1)}, u32[]{:S(2)}) copy-start(bf16[256,2048]{1,0:T(8,128)(2,1)} %param.22) | copy-start | bytes 3145732
  46.6 23.4 %collective-permute-start.2 = (bf16[256,2048]{1,0:T(8,128)(2,1)S(1)}, bf16[256,2048]{1,0:T(8,128)(2,1)}, u32[]{:S(2)}, u32[]{:S(2)}) collective-permute-start(bf16[256,2048]{1,0:T(8,128)(2,1)S(1)} %dynamic-slice_convert_fusion), channel_id=1, source_target_pairs={{0,1},{1,0},{2,3},{3,2},{4,5},{5,4},{6,7},{7,6},{8,9},{9,8},{10,11... | collective-permute-start | bytes 3145736 | tf_op jit(solution)/shard_map/ppermute | solution.py:163
  47.8 24.7 %copy-start.15 = (f32[2048]{0:T(1024)S(1)}, f32[2048]{0:T(1024)}, u32[]{:S(2)}) copy-start(f32[2048]{0:T(1024)} %param.23) | copy-start | bytes 24580
  72.8 3.1 copy-start.14
  73.8 135.1 %all-gather.9.cloned.1.call-start = ((), (), s32[]{:S(2)}) async-start(), calls=%async_computation.7 | async-start | bytes 4456448 | tf_op jit(solution)/shard_map/all_gather | solution.py:218
  74.6 204.8 %all-gather.7.cloned.1.call-start = ((), (), s32[]{:S(2)}) async-start(), calls=%async_computation.6 | async-start | bytes 4456448 | tf_op jit(solution)/shard_map/all_gather | solution.py:218
  75.3 290.2 %all-gather.11.cloned.1.call-start = ((), (), s32[]{:S(2)}) async-start(), calls=%async_computation.9 | async-start | bytes 4456448 | tf_op jit(solution)/shard_map/all_gather | solution.py:218
  75.9 4.0 copy-start.16
  76.0 4.0 copy-start.17
  78.7 13.6 %collective-permute-start.3 = (bf16[96,2048]{1,0:T(8,128)(2,1)S(1)}, bf16[96,2048]{1,0:T(8,128)(2,1)S(1)}, u32[]{:S(2)}, u32[]{:S(2)}) collective-permute-start(bf16[96,2048]{1,0:T(8,128)(2,1)S(1)} %pad_maximum_fusion.1), channel_id=1, source_target_pairs={{0,1},{1,0},{2,3},{3,2},{4,5},{5,4},{6,7},{7,6},{8,9},{9,8},{10,11... | collective-permute-start | bytes 1179656 | tf_op jit(solution)/shard_map/ppermute | solution.py:148
  80.6 11.1 %all-to-all-start = ((f32[16,1,256]{2,1,0:T(1,128)}), f32[16,1,256]{2,1,0:T(1,128)S(1)}, u32[]{:S(2)}, u32[]{:S(2)}) async-start(f32[16,1,256]{2,1,0:T(1,128)} %copy.95), calls=%async_computation | async-start | bytes 32768 | tf_op jit(solution)/shard_map/all_to_all | solution.py:213
  125.1 1.6 copy-start.2
  142.6 154.2 %all-to-all-start.1 = ((bf16[16,64,2048]{2,1,0:T(8,128)(2,1)}), bf16[16,64,2048]{2,1,0:T(8,128)(2,1)}, u32[]{:S(2)}, u32[]{:S(2)}) async-start(bf16[16,64,2048]{2,1,0:T(8,128)(2,1)} %bitcast.57), calls=%async_computation.1 | async-start | bytes 8388608 | tf_op jit(solution)/shard_map/all_to_all | solution.py:224
  148.2 300.8 %reduce-scatter.3.cloned.1.call-start = ((), (), s32[]{:S(2)}) async-start(), calls=%async_computation.8 | async-start | bytes 4456448 | tf_op jit(solution)/shard_map/reduce_scatter | solution.py:228
  209.0 1.6 copy-start.3
  279.4 1.6 copy-start.4
  296.7 233.4 %all-to-all-start.2 = ((bf16[16,64,2048]{2,1,0:T(8,128)(2,1)}), bf16[16,64,2048]{2,1,0:T(8,128)(2,1)}, u32[]{:S(2)}, u32[]{:S(2)}) async-start(bf16[16,64,2048]{2,1,0:T(8,128)(2,1)} %bitcast.56), calls=%async_computation.2 | async-start | bytes 8388608 | tf_op jit(solution)/shard_map/all_to_all | solution.py:224
  304.7 219.9 %reduce-scatter.5.cloned.1.call-start = ((), (), s32[]{:S(2)}) async-start(), calls=%async_computation.10 | async-start | bytes 4456448 | tf_op jit(solution)/shard_map/reduce_scatter | solution.py:228
  365.5 1.6 copy-start.5
  530.2 3.2 copy-start.8
  530.2 3.2 copy-start.9
  530.2 3.2 copy-start.10
  530.2 4.5 copy-start.1
Sparse Core Ops, SparseCore 0:
  74.0 51.1 all-gather.4
  127.3 81.6 all-gather.8
  211.2 68.1 all-gather.6
  281.4 84.0 all-gather.10
  369.2 79.6 reduce-scatter.2
  452.6 71.8 reduce-scatter.4
